TPU v7x, 32 devices: a whole 2x2x4 slice. The times are simulated.
32 devices in a mesh: sp: 4 (over z), tp: 2 (over y), dp: 4 (over x, core).
Axes of the slice: x: 2, y: 2, z: 4, core: 2. Of those that a mesh axis runs over, the one named last changes fastest.
Arguments:
- latent: bfloat16 [2048, 2048], P(('dp', 'sp', 'tp')), parts along dimension 0, may hold values from -6 to 6
- cond: bfloat16 [8192], P('dp'), parts along dimension 0, may hold values from -6 to 6
- context: bfloat16 [2048, 2048], P(('dp', 'sp')), parts along dimension 0, may hold values from -6 to 6
- context_cond: bfloat16 [2048], replicated, may hold values from -6 to 6
- modulation: bfloat16 [2048, 6144], P(('sp', 'tp')), may hold values from -0.125 to 0.125
- norm_gain: bfloat16 [2048], replicated, may hold values from 0.099609375 to 1.8984375
- w_x: bfloat16 [2048, 1024], P(None, 'tp'), may hold values from -0.125 to 0.125
- w_gate: bfloat16 [2048, 1024], P(None, 'tp'), may hold values from -0.125 to 0.125
- w_b: bfloat16 [2048, 256], P(None, 'tp'), may hold values from -0.125 to 0.125
- w_c: bfloat16 [2048, 256], P(None, 'tp'), may hold values from -0.125 to 0.125
- w_dt: bfloat16 [2, 2048, 16], P(None, None, 'tp'), may hold values from -0.125 to 0.125
- conv_x: bfloat16 [4, 1024], P(None, 'tp'), may hold values from -3 to 3
- conv_b: bfloat16 [4, 256], P(None, 'tp'), may hold values from -3 to 3
- conv_c: bfloat16 [4, 256], P(None, 'tp'), may hold values from -3 to 3
- decay_rate: float32 [2, 16], P(None, 'tp'), may hold values from 0 to 0.04
- decay_extra: float32 [2048, 16], P(('dp', 'sp'), 'tp'), parts along dimension 0, may hold values from -2 to 0
- out_gain: bfloat16 [1024], P('tp'), may hold values from 0.099609375 to 1.8984375
- w_out: bfloat16 [1024, 2048], replicated, may hold values from -0.1875 to 0.1875
Outputs:
- mixed: bfloat16 [2048, 2048], P(('dp', 'sp', 'tp')), parts along dimension 0
There are 4 independent parts, one for each index of `dp`. A program takes and returns all parts, laid end to end along the dimension named above; an argument that names none is the same for every part. Nothing has to cross between parts.
All inputs are finite; a program needn't handle non-finite values.
Results may differ from a plain program's by a relative error of at most 0.007.
Values may be sent and summed in bfloat16 or wider, within the bound.
A program may use at most 64 MiB of HBM per device.

v0:
```python
import jax
import jax.numpy as jnp
from jax import lax
from jax.sharding import PartitionSpec as P

HEAD_DIM = 64
STATE = 64
BLOCK = 128
ROW_EPS = 1e-06
GROUP_EPS = 1e-05
HIGHEST = lax.Precision.HIGHEST


def prefix(x, axis, join, neutral, backward):
    count = lax.axis_size(axis)
    place = lax.axis_index(axis)
    ahead = count - 1 - place if backward else place
    gathered = jax.tree.map(
        lambda a, kind: lax.all_gather(a.astype(kind), axis),
        x,
        jax.tree.map(lambda a: jnp.bfloat16 if a.dtype == jnp.float32 else a.dtype, x),
    )
    state = jax.tree.map(lambda a, e: jnp.zeros_like(a) + jnp.asarray(e, a.dtype), x, neutral)

    def one(hop, state):
        source = count - 1 - hop if backward else hop
        return join(
            state,
            jax.tree.map(
                lambda a, own: lax.dynamic_index_in_dim(a, source, 0, False).astype(own.dtype),
                gathered,
                x,
            ),
        )

    return lax.fori_loop(0, ahead, one, state)


def with_halo(block, sides, width):
    for axis, dim in sides:
        count = lax.axis_size(axis)
        forward = [(i, i + 1) for i in range(count - 1)]
        backward = [(target, source) for source, target in forward]
        low = lax.ppermute(
            lax.slice_in_dim(block, block.shape[dim] - width, None, axis=dim), axis, forward
        )
        high = lax.ppermute(lax.slice_in_dim(block, 0, width, axis=dim), axis, backward)
        block = jnp.concatenate([low, block, high], axis=dim)
    return block


def modulated_norm(row_block, norm_gain, shift_row, scale_row):
    values = row_block.astype(jnp.float32)
    normed = values * lax.rsqrt(jnp.mean(values * values, axis=-1, keepdims=True) + ROW_EPS)
    return (normed * norm_gain.astype(jnp.float32) * (1.0 + scale_row) + shift_row).astype(
        jnp.bfloat16
    )


def project_many(row_block, weights):
    return jnp.concatenate(
        [
            jnp.dot(row_block, weight, preferred_element_type=jnp.float32).astype(jnp.bfloat16)
            for weight in weights
        ],
        axis=1,
    )


def conv_padded(padded, conv_taps, length):
    values = padded.astype(jnp.float32)
    summed = jnp.zeros((length, values.shape[1]), jnp.float32)
    for offset in range(conv_taps.shape[0]):
        summed = summed + conv_taps[offset].astype(jnp.float32) * values[offset : offset + length]
    return jax.nn.silu(summed).astype(jnp.bfloat16)


def context_states(ctx_xs, ctx_bmat, ctx_dt, decay_rate):
    length = ctx_xs.shape[0]
    groups = ctx_bmat.shape[1] // STATE
    heads_here = ctx_dt.shape[2]
    repeat = heads_here // groups
    values = ctx_xs.astype(jnp.float32).reshape(length, groups, repeat, HEAD_DIM)
    keys_b = ctx_bmat.astype(jnp.float32).reshape(length, groups, STATE)
    log_decay = -decay_rate[:, None, :] * ctx_dt
    running = jnp.cumsum(log_decay, axis=1)
    forward_weight = (jnp.exp(running[0, -1:] - running[0]) * ctx_dt[0]).reshape(
        length, groups, repeat
    )
    backward_weight = (jnp.exp(running[1] - log_decay[1]) * ctx_dt[1]).reshape(
        length, groups, repeat
    )
    forward_state = jnp.einsum(
        "lgn,lgr,lgrp->grpn", keys_b, forward_weight, values, precision=HIGHEST
    )
    backward_state = jnp.einsum(
        "lgn,lgr,lgrp->grpn", keys_b, backward_weight, values, precision=HIGHEST
    )
    return (forward_state, backward_state)


def block_pass(inputs, step_sizes, log_decay, bmat, cmat, start_state):
    length = inputs.shape[0]
    groups, repeat = (start_state.shape[0], start_state.shape[1])
    block_count = length // BLOCK
    values = inputs.reshape(block_count, BLOCK, groups, repeat, HEAD_DIM)
    steps_blk = step_sizes.reshape(block_count, BLOCK, groups, repeat)
    decays = log_decay.reshape(block_count, BLOCK, groups, repeat)
    keys_b = bmat.reshape(block_count, BLOCK, groups, STATE)
    reads_c = cmat.reshape(block_count, BLOCK, groups, STATE)
    lower_mask = (jnp.arange(BLOCK)[:, None] >= jnp.arange(BLOCK)[None, :])[:, :, None, None]

    def advance(carried, block_data):
        value_blk, step_blk, decay_blk, key_blk, read_blk = block_data
        running = jnp.cumsum(decay_blk, axis=0)
        log_gaps = running[:, None] - running[None, :]
        mixing = jnp.where(lower_mask, jnp.exp(jnp.where(lower_mask, log_gaps, 0.0)), 0.0)
        affinity = jnp.einsum("ign,jgn->ijg", read_blk, key_blk, preferred_element_type=jnp.float32)
        weights = (affinity[..., None] * mixing * step_blk[None]).astype(jnp.bfloat16)
        output = jnp.einsum(
            "ijgr,jgrp->igrp", weights, value_blk, preferred_element_type=jnp.float32
        )
        output = output + jnp.einsum(
            "ign,grpn,igr->igrp",
            read_blk.astype(jnp.float32),
            carried,
            jnp.exp(running),
            precision=HIGHEST,
        )
        to_end = jnp.exp(running[-1:] - running) * step_blk
        state_in = (key_blk.astype(jnp.float32)[:, :, None, :] * to_end[..., None]).astype(
            jnp.bfloat16
        )
        carried = jnp.exp(running[-1])[..., None, None] * carried + jnp.einsum(
            "jgrn,jgrp->grpn", state_in, value_blk, preferred_element_type=jnp.float32
        )
        return (carried, output)

    final_state, outputs = lax.scan(
        advance, start_state, (values, steps_blk, decays, keys_b, reads_c)
    )
    return (outputs.reshape(length, groups, repeat, HEAD_DIM), final_state)


def state_chain(summary, backward):

    def combine(earlier, later_part):
        return (
            earlier[0] + later_part[0],
            jnp.exp(later_part[0])[..., None, None] * earlier[1] + later_part[1],
        )

    identity_pair = (jnp.zeros_like(summary[0]), jnp.zeros_like(summary[1]))
    return prefix(summary, "sp", combine, identity_pair, backward)


def directed_pass(inputs, step_sizes, log_decay, bmat, cmat, outer_start, zeros_state, backward):
    local_out, final_state = block_pass(inputs, step_sizes, log_decay, bmat, cmat, zeros_state)
    length = inputs.shape[0]
    groups, repeat = (zeros_state.shape[0], zeros_state.shape[1])
    running = jnp.cumsum(log_decay, axis=0).reshape(length, groups, repeat)
    before = state_chain((running[-1], final_state), backward)
    entry_state = jnp.exp(before[0])[..., None, None] * outer_start + before[1]
    read_rows = cmat.astype(jnp.float32).reshape(length, groups, STATE)
    return local_out + jnp.einsum(
        "tgn,grpn,tgr->tgrp", read_rows, entry_state, jnp.exp(running), precision=HIGHEST
    )


def group_norm(combined, out_gain):
    length, groups, repeat, _ = combined.shape
    mean_square = jnp.mean(combined * combined, axis=(2, 3), keepdims=True)
    scaled = (
        combined
        * lax.rsqrt(mean_square + GROUP_EPS)
        * out_gain.astype(jnp.float32).reshape(groups, repeat, HEAD_DIM)
    )
    return scaled.reshape(length, groups * repeat * HEAD_DIM).astype(jnp.bfloat16)


def local(
    latent,
    cond,
    context,
    context_cond,
    modulation,
    norm_gain,
    w_x,
    w_gate,
    w_b,
    w_c,
    w_dt,
    conv_x,
    conv_b,
    conv_c,
    decay_rate,
    decay_extra,
    out_gain,
    w_out,
):
    model_width = latent.shape[1]
    mod_share = modulation.shape[0]
    cond_rows = jax.nn.silu(jnp.stack([cond, context_cond]).astype(jnp.float32)).astype(
        jnp.bfloat16
    )
    own_cols = lax.dynamic_slice_in_dim(
        cond_rows, lax.axis_index(("sp", "tp")) * mod_share, mod_share, 1
    )
    mod_rows = lax.psum(
        jnp.dot(own_cols, modulation, preferred_element_type=jnp.float32), ("sp", "tp")
    )
    shift_rows = mod_rows[:, :model_width]
    scale_rows = mod_rows[:, model_width : 2 * model_width]
    gate_row = mod_rows[0, 2 * model_width :]
    head_cols = w_x.shape[1]
    state_cols = w_b.shape[1]
    heads_here = w_dt.shape[2]
    groups_here = state_cols // STATE
    repeat = heads_here // groups_here
    hidden = modulated_norm(latent, norm_gain, shift_rows[0], scale_rows[0])
    latent_mats = (w_x, w_b, w_c, w_gate, w_dt[0], w_dt[1])
    projected = project_many(lax.all_gather(hidden, "tp", axis=0, tiled=True), latent_mats)
    token_count = projected.shape[0]
    conv_cols = head_cols + 2 * state_cols
    extended = with_halo(projected[:, :conv_cols], (("sp", 0),), 2)
    conv_taps = jnp.concatenate([conv_x, conv_b, conv_c], axis=1)
    convolved = conv_padded(extended, conv_taps, token_count)
    latent_xs = convolved[:, :head_cols]
    latent_b = convolved[:, head_cols : head_cols + state_cols]
    latent_c = convolved[:, head_cols + state_cols :]
    gate_in = projected[:, conv_cols : conv_cols + head_cols]
    dt_start = conv_cols + head_cols
    latent_dt = jnp.stack(
        [
            jax.nn.softplus(projected[:, dt_start : dt_start + heads_here].astype(jnp.float32)),
            jax.nn.softplus(projected[:, dt_start + heads_here :].astype(jnp.float32)),
        ]
    )
    context_mats = (w_x, w_b, w_dt[0], w_dt[1])
    own_context = project_many(
        modulated_norm(context, norm_gain, shift_rows[1], scale_rows[1]), context_mats
    )
    context_cols = lax.all_gather(own_context, "sp", axis=0, tiled=True)
    ctx_span = head_cols + state_cols
    ctx_padded = jnp.pad(context_cols[:, :ctx_span], ((2, 1), (0, 0)))
    ctx_conv = conv_padded(
        ctx_padded, jnp.concatenate([conv_x, conv_b], axis=1), context_cols.shape[0]
    )
    ctx_dt = jnp.stack(
        [
            jax.nn.softplus(context_cols[:, ctx_span : ctx_span + heads_here].astype(jnp.float32)),
            jax.nn.softplus(context_cols[:, ctx_span + heads_here :].astype(jnp.float32)),
        ]
    )
    forward_start, backward_start = context_states(
        ctx_conv[:, :head_cols], ctx_conv[:, head_cols:], ctx_dt, decay_rate
    )
    log_decay = -decay_rate[:, None, :] * latent_dt + decay_extra[None]
    zeros_state = jnp.zeros((groups_here, repeat, HEAD_DIM, STATE), jnp.float32)
    y_forward = directed_pass(
        latent_xs, latent_dt[0], log_decay[0], latent_b, latent_c, forward_start, zeros_state, False
    )
    y_backward = directed_pass(
        latent_xs[::-1],
        latent_dt[1][::-1],
        log_decay[1][::-1],
        latent_b[::-1],
        latent_c[::-1],
        backward_start,
        zeros_state,
        True,
    )
    gate_act = jax.nn.silu(gate_in.astype(jnp.float32)).reshape(
        token_count, groups_here, repeat, HEAD_DIM
    )
    combined = (y_forward + y_backward[::-1]) * gate_act
    normed = group_norm(combined, out_gain)
    tp_count = lax.axis_size("tp")
    stacked = normed.reshape(tp_count, token_count // tp_count, normed.shape[1])
    branch = jnp.dot(
        lax.all_to_all(stacked, "tp", split_axis=0, concat_axis=2, tiled=True)[0],
        w_out,
        preferred_element_type=jnp.float32,
    )[None]
    return (latent.astype(jnp.float32) + gate_row * branch[0]).astype(jnp.bfloat16)


def solution(mesh):
    in_specs = (
        P(("dp", "sp", "tp"), None),
        P("dp"),
        P(("dp", "sp"), None),
        P(),
        P(("sp", "tp"), None),
        P(),
        P(None, "tp"),
        P(None, "tp"),
        P(None, "tp"),
        P(None, "tp"),
        P(None, None, "tp"),
        P(None, "tp"),
        P(None, "tp"),
        P(None, "tp"),
        P(None, "tp"),
        P(("dp", "sp"), "tp"),
        P("tp"),
        P(),
    )
    out_specs = P(("dp", "sp", "tp"), None)
    return jax.shard_map(local, mesh=mesh, in_specs=in_specs, out_specs=out_specs, check_vma=False)
```

profile of v0, /device:TPU:0, one launch (start us, length us, event | category | flops | bytes accessed | tf_op | source)
XLA Modules:
  0.0 247.8 jit_solution(15845269503590403432)
XLA Ops:
  2.4 39.4 %psum.7 = f32[2,6144]{1,0:T(2,128)S(1)} all-reduce(f32[2,6144]{1,0:T(2,128)S(1)} %fusion.93), channel_id=1, replica_groups=mesh['sp'=4,'tp'=2,'dp'=4] {'sp','tp'}, use_global_device_ids=true, to_apply=%region_0.1 | all-reduce | flops 12288 | bytes 98304 | tf_op jit(solution)/shard_map/psum | solution.py:209
  42.9 7.2 %all_gather.26 = bf16[128,2048]{1,0:T(8,128)(2,1)S(1)} all-gather(bf16[64,2048]{1,0:T(8,128)(2,1)S(1)} %fusion.31), channel_id=1, replica_groups=mesh['sp'=4,'tp'=2,'dp'=4] {'tp'}, dimensions={0}, use_global_device_ids=true | all-gather | bytes 786432 | tf_op jit(solution)/shard_map/all_gather | solution.py:222
  50.0 2.3 convolution_convert_fusion.2
  53.6 1.9 collective-permute-start
  55.4 1.3 collective-permute-start.1
  60.7 2.9 %convolution_convert_fusion.1 = bf16[128,512]{0,1:T(8,128)(2,1)S(1)} fusion(bf16[2048,512]{1,0:T(8,128)(2,1)} %param.28, bf16[128,2048]{1,0:T(8,128)(2,1)} %param.24, f32[2048]{0:T(1024)} %bitcast.249, f32[2048]{0:T(1024)} %bitcast.253, f32[2048]{0:T(1024)S(1)} %convert_element_type.221, f32[128]{0:T(128)S(1)} %add_rsqrt_fusion.1), kind=kOutput, calls=%fused_computation.49 | convolution fusion | flops 270073856 | bytes 2777600 | tf_op jit(solution)/shard_map/dot_general | solution.py:63
  65.2 14.5 %all_gather.30 = bf16[512,656]{0,1:T(8,128)(2,1)S(1)} all-gather(bf16[128,656]{0,1:T(8,128)(2,1)S(1)} %pad_maximum_fusion), channel_id=1, replica_groups=mesh['sp'=4,'tp'=2,'dp'=4] {'sp'}, dimensions={0}, use_global_device_ids=true | all-gather | bytes 839680 | tf_op jit(solution)/shard_map/all_gather | solution.py:243
  90.8 1.6 reduce_window_sum.52
  93.7 5.0 %reduce-window.6 = f32[2,8,4,128]{3,1,2,0:T(8,128)} reduce-window(f32[2,8,4,128]{3,1,2,0:T(8,128)} %fusion.148, f32[]{:T(128)} %constant.128.clone.1), window={size=1x1x1x128 pad=0_0x0_0x0_0x127_0}, to_apply=%region_7.8 | reduce-window | flops 1040384 | bytes 65540 | tf_op jit(solution)/shard_map/reduce-window
  98.7 1.5 slice_reduce_fusion
  103.1 2.7 %pad_convert_fusion = f32[515,640]{0,1:T(8,128)} fusion(bf16[512,640]{0,1:T(8,128)(2,1)} %slice.222), kind=kLoop, calls=%fused_computation.67 | loop fusion | flops 329600 | bytes 1973760 | tf_op jit(solution)/shard_map/convert_element_type | solution.py:71
  107.2 1.6 reduce_window_sum.56
  110.2 3.1 %divide_multiply_fusion = f32[128,512]{1,0:T(8,128)} fusion(bf16[128,2048]{1,0:T(8,128)(2,1)} %copy-done.2, bf16[2048,512]{1,0:T(8,128)(2,1)} %param.29), kind=kOutput, calls=%fused_computation.89 | convolution fusion | flops 268828672 | bytes 2883584 | tf_op jit(solution)/shard_map/dot_general | solution.py:63
  113.3 1.4 fusion.76
  116.3 2.4 multiply_convert_fusion
  118.7 10.4 %all_gather.27 = bf16[4,2,4]{2,1,0:T(2,128)(2,1)} all-gather(bf16[1,2,4]{2,1,0:T(2,128)(2,1)S(1)} %copy-done.55), channel_id=1, replica_groups=mesh['sp'=4,'tp'=2,'dp'=4] {'sp'}, dimensions={0}, use_global_device_ids=true | all-gather | bytes 80 | tf_op jit(solution)/shard_map/all_gather | solution.py:19
  129.1 8.0 %all_gather.31 = bf16[4,2,4]{2,1,0:T(2,128)(2,1)} all-gather(bf16[1,2,4]{2,1,0:T(2,128)(2,1)S(1)} %copy-done.56), channel_id=1, replica_groups=mesh['sp'=4,'tp'=2,'dp'=4] {'sp'}, dimensions={0}, use_global_device_ids=true | all-gather | bytes 80 | tf_op jit(solution)/shard_map/all_gather | solution.py:19
  137.1 1.9 slice.230
  139.0 1.6 slice.231
  140.5 1.5 exp.128
  142.0 1.5 exp.139
  145.8 1.4 reshape.201
  147.2 1.5 copy.174
  148.7 1.3 reshape.203
  150.0 1.6 copy.189
  151.6 1.5 copy.187
  153.1 1.6 copy.185
  154.6 1.6 copy.172
  156.2 1.8 copy.190
  158.0 1.3 reshape.218
  160.6 1.3 rev.18
  164.3 16.6 %all-gather = bf16[8,4,64,64]{3,2,1,0:T(8,128)(2,1)} all-gather(bf16[2,4,64,64]{3,2,1,0:T(8,128)(2,1)S(1)} %fusion.17), channel_id=2, replica_groups=mesh['sp'=4,'tp'=2,'dp'=4] {'sp'}, dimensions={0}, use_global_device_ids=true | all-gather | bytes 327680 | tf_op jit(solution)/shard_map/all_gather | solution.py:19
  182.7 1.6 copy.178
  184.3 1.5 copy.179
  187.7 19.2 %all-gather.1 = bf16[8,4,64,64]{3,2,1,0:T(8,128)(2,1)} all-gather(bf16[2,4,64,64]{3,2,1,0:T(8,128)(2,1)S(1)} %fusion.18), channel_id=3, replica_groups=mesh['sp'=4,'tp'=2,'dp'=4] {'sp'}, dimensions={0}, use_global_device_ids=true | all-gather | bytes 327680 | tf_op jit(solution)/shard_map/all_gather | solution.py:19
  207.5 7.0 %while.7 = (s32[]{:T(128)}, f32[2,4]{1,0:T(2,128)}, f32[2,4,64,64]{3,2,1,0:T(8,128)S(1)}, s32[]{:T(128)}, bf16[4,2,4]{2,1,0:T(2,128)(2,1)}, /*index=5*/bf16[4,2,...) while((s32[]{:T(128)}, f32[2,4]{1,0:T(2,128)}, f32[2,4,64,64]{3,2,1,0:T(8,128)S(1)}, ...), condition=%wide.region_12.13_spmd, body=%wide.region_11.12_spmd.sunk | while | flops 98326 | bytes 327979 | solution.py:36
  209.7 1.3 convert_exponential_fusion.5
  214.5 1.3 exp.143
  215.8 1.5 copy.180
  217.2 1.6 convolution_bitcast_fusion.6
  218.9 1.6 copy.181
  221.6 1.7 fusion.15
  225.5 1.8 rev.23
  227.3 1.6 convolution_bitcast_fusion.7
  229.0 1.7 copy.168
  231.7 1.7 fusion.16
  237.0 6.8 %all_to_all.15 = bf16[2,64,512]{2,1,0:T(8,128)(2,1)S(1)} all-to-all(bf16[2,64,512]{2,1,0:T(8,128)(2,1)S(1)} %copy.199), channel_id=1, replica_groups=mesh['sp'=4,'tp'=2,'dp'=4] {'tp'}, dimensions={0} | all-to-all | bytes 262144 | tf_op jit(solution)/shard_map/all_to_all | solution.py:281
  244.1 3.8 %fusion.1 = bf16[64,2048]{1,0:T(8,128)(2,1)} fusion(bf16[64,1024]{1,0:T(8,128)(2,1)S(1)} %bitcast.213, bf16[1024,2048]{1,0:T(8,128)(2,1)} %param.39, bf16[64,2048]{1,0:T(8,128)(2,1)S(1)} %copy-done.7, f32[2048]{0:T(1024)S(1)} %bitcast.239), kind=kOutput, calls=%fused_computation.10 | convolution fusion | flops 268959744 | bytes 4857856 | tf_op jit(solution)/shard_map/dot_general | solution.py:280
  (214 shorter events, 53.2 us)
Async XLA Ops:
  1.9 40.6 %copy-start.48 = (bf16[2048]{0:T(1024)(128)(2,1)S(1)}, bf16[2048]{0:T(1024)(128)(2,1)}, u32[]{:S(2)}) copy-start(bf16[2048]{0:T(1024)(128)(2,1)} %param.27) | copy-start | bytes 12292
  1.9 40.6 %copy-start.6 = (bf16[64,2048]{1,0:T(8,128)(2,1)S(1)}, bf16[64,2048]{1,0:T(8,128)(2,1)}, u32[]{:S(2)}) copy-start(bf16[64,2048]{1,0:T(8,128)(2,1)} %param.22) | copy-start | bytes 786436
  42.8 9.4 %copy-start.11 = (bf16[2048,128]{1,0:T(8,128)(2,1)S(1)}, bf16[2048,128]{1,0:T(8,128)(2,1)}, u32[]{:S(2)}) copy-start(bf16[2048,128]{1,0:T(8,128)(2,1)} %param.31) | copy-start | bytes 1572868
  50.0 7.0 %copy-start.2 = (bf16[128,2048]{1,0:T(8,128)(2,1)}, bf16[128,2048]{1,0:T(8,128)(2,1)S(1)}, u32[]{:S(2)}) copy-start(bf16[128,2048]{1,0:T(8,128)(2,1)S(1)} %all_gather.26) | copy-start | bytes 1572868
  52.3 4.4 %copy-start.27 = (bf16[2,2048,8]{1,2,0:T(8,128)(2,1)S(1)}, bf16[2,2048,8]{1,2,0:T(8,128)(2,1)}, u32[]{:S(2)}) copy-start(bf16[2,2048,8]{1,2,0:T(8,128)(2,1)} %param.32) | copy-start | bytes 196612
  52.3 4.9 %copy-start.54 = (f32[2,8]{1,0:T(2,128)S(1)}, f32[2,8]{1,0:T(2,128)}, u32[]{:S(2)}) copy-start(f32[2,8]{1,0:T(2,128)} %param.36) | copy-start | bytes 196
  52.3 5.0 %copy-start.52 = (f32[128,8]{0,1:T(8,128)S(1)}, f32[128,8]{0,1:T(8,128)}, u32[]{:S(2)}) copy-start(f32[128,8]{0,1:T(8,128)} %param.37) | copy-start | bytes 12292
  52.6 5.3 %copy-start.18 = (bf16[128,128]{1,0:T(8,128)(2,1)}, bf16[128,128]{1,0:T(8,128)(2,1)S(1)}, u32[]{:S(2)}) copy-start(bf16[128,128]{1,0:T(8,128)(2,1)S(1)} %convolution_convert_fusion.4) | copy-start | bytes 98308
  52.9 5.0 %copy-start.19 = (bf16[128,128]{1,0:T(8,128)(2,1)}, bf16[128,128]{1,0:T(8,128)(2,1)S(1)}, u32[]{:S(2)}) copy-start(bf16[128,128]{1,0:T(8,128)(2,1)S(1)} %convolution_convert_fusion.5) | copy-start | bytes 98308
  53.6 105.8 %collective-permute-start = (bf16[2,768]{1,0:T(2,128)(2,1)}, bf16[2,768]{1,0:T(2,128)(2,1)}, u32[]{:S(2)}, u32[]{:S(2)}) collective-permute-start(bf16[2,768]{1,0:T(2,128)(2,1)} %get-tuple-element.220), channel_id=1, source_target_pairs={{0,8},{8,16},{16,24},{1,9},{9,17},{17,25},{2,10},{10,18},{18,26},{... | collective-permute-start | bytes 9224 | tf_op jit(solution)/shard_map/ppermute | solution.py:44
  55.4 103.9 %collective-permute-start.1 = (bf16[2,768]{1,0:T(2,128)(2,1)}, bf16[2,768]{1,0:T(2,128)(2,1)}, u32[]{:S(2)}, u32[]{:S(2)}) collective-permute-start(bf16[2,768]{1,0:T(2,128)(2,1)} %get-tuple-element.221), channel_id=1, source_target_pairs={{8,0},{16,8},{24,16},{9,1},{17,9},{25,17},{10,2},{18,10},{26,18},{... | collective-permute-start | bytes 9224 | tf_op jit(solution)/shard_map/ppermute | solution.py:47
  57.0 29.6 %copy-start.25 = (f32[128,8]{0,1:T(8,128)}, f32[128,8]{0,1:T(8,128)S(1)}, u32[]{:S(2)}) copy-start(f32[128,8]{0,1:T(8,128)S(1)} %compare_select_fusion.3) | copy-start | bytes 12292
  64.8 14.9 %copy-start.37 = (f32[2,8]{1,0:T(2,128)S(1)}, f32[2,8]{1,0:T(2,128)}, u32[]{:S(2)}) copy-start(f32[2,8]{1,0:T(2,128)} %copy-done.36) | copy-start | bytes 196
  65.2 17.6 %copy-start.41 = (f32[128,8]{0,1:T(8,128)S(1)}, f32[128,8]{0,1:T(8,128)}, u32[]{:S(2)}) copy-start(f32[128,8]{0,1:T(8,128)} %get-tuple-element.233) | copy-start | bytes 12292
  65.2 24.9 %copy-start.38 = (f32[128,8]{0,1:T(8,128)S(1)}, f32[128,8]{0,1:T(8,128)}, u32[]{:S(2)}) copy-start(f32[128,8]{0,1:T(8,128)} %get-tuple-element.232) | copy-start | bytes 12292
  100.9 5.5 %copy-start.39 = (f32[128,8]{0,1:T(8,128)S(1)}, f32[128,8]{0,1:T(8,128)}, u32[]{:S(2)}) copy-start(f32[128,8]{0,1:T(8,128)} %rev.22) | copy-start | bytes 12292
  110.2 3.2 %copy-start.22 = (f32[2,512,8]{1,2,0:T(8,128)S(1)}, f32[2,512,8]{1,2,0:T(8,128)}, u32[]{:S(2)}) copy-start(f32[2,512,8]{1,2,0:T(8,128)} %copy-done.21) | copy-start | bytes 98308
  110.2 3.2 %copy-start.24 = (f32[2,512,8]{1,2,0:T(8,128)S(1)}, f32[2,512,8]{1,2,0:T(8,128)}, u32[]{:S(2)}) copy-start(f32[2,512,8]{1,2,0:T(8,128)} %maximum_multiply_fusion) | copy-start | bytes 98308
  110.2 3.2 %copy-start.53 = (f32[8]{0:T(128)S(1)}, f32[8]{0:T(128)}, u32[]{:S(2)}) copy-start(f32[8]{0:T(128)} %slice_reduce_fusion.1) | copy-start | bytes 100
  110.2 4.6 %copy-start.50 = (f32[2,4]{1,0:T(2,128)S(1)}, f32[2,4]{1,0:T(2,128)}, u32[]{:S(2)}) copy-start(f32[2,4]{1,0:T(2,128)} %slice_bitcast_fusion.3) | copy-start | bytes 100
  110.2 4.6 %copy-start.15 = (f32[128,2,4]{2,1,0:T(2,128)S(1)}, f32[128,2,4]{2,1,0:T(2,128)}, u32[]{:S(2)}) copy-start(f32[128,2,4]{2,1,0:T(2,128)} %copy.175) | copy-start | bytes 12292
  110.2 5.3 %copy-start.51 = (f32[2,4]{1,0:T(2,128)S(1)}, f32[2,4]{1,0:T(2,128)}, u32[]{:S(2)}) copy-start(f32[2,4]{1,0:T(2,128)} %slice_bitcast_fusion.2) | copy-start | bytes 100
  110.2 5.3 %copy-start.16 = (f32[128,2,4]{2,1,0:T(2,128)S(1)}, f32[128,2,4]{2,1,0:T(2,128)}, u32[]{:S(2)}) copy-start(f32[128,2,4]{2,1,0:T(2,128)} %copy.188) | copy-start | bytes 12292
  110.2 6.1 %copy-start.1 = (f32[515,640]{0,1:T(8,128)S(1)}, f32[515,640]{0,1:T(8,128)}, u32[]{:S(2)}) copy-start(f32[515,640]{0,1:T(8,128)} %pad_convert_fusion) | copy-start | bytes 3955204
  110.2 6.1 %copy-start.42 = (f32[640]{0:T(1024)S(1)}, f32[640]{0:T(1024)}, u32[]{:S(2)}) copy-start(f32[640]{0:T(1024)} %get-tuple-element.183) | copy-start | bytes 7684
  110.2 6.1 %copy-start.43 = (f32[640]{0:T(1024)S(1)}, f32[640]{0:T(1024)}, u32[]{:S(2)}) copy-start(f32[640]{0:T(1024)} %get-tuple-element.184) | copy-start | bytes 7684
  110.2 6.1 %copy-start.44 = (f32[640]{0:T(1024)S(1)}, f32[640]{0:T(1024)}, u32[]{:S(2)}) copy-start(f32[640]{0:T(1024)} %get-tuple-element.185) | copy-start | bytes 7684
  116.3 12.8 %copy-start.56 = (bf16[1,2,4]{2,1,0:T(2,128)(2,1)S(1)}, bf16[1,2,4]{2,1,0:T(2,128)(2,1)}, u32[]{:S(2)}) copy-start(bf16[1,2,4]{2,1,0:T(2,128)(2,1)} %convert_element_type.248) | copy-start | bytes 52
  144.2 16.0 %copy-start.31 = (f32[768]{0:T(1024)S(1)}, f32[768]{0:T(1024)}, u32[]{:S(2)}) copy-start(f32[768]{0:T(1024)} %get-tuple-element.178) | copy-start | bytes 9220
  144.2 16.0 %copy-start.32 = (f32[768]{0:T(1024)S(1)}, f32[768]{0:T(1024)}, u32[]{:S(2)}) copy-start(f32[768]{0:T(1024)} %get-tuple-element.179) | copy-start | bytes 9220
  144.2 16.0 %copy-start.33 = (f32[768]{0:T(1024)S(1)}, f32[768]{0:T(1024)}, u32[]{:S(2)}) copy-start(f32[768]{0:T(1024)} %get-tuple-element.180) | copy-start | bytes 9220
  144.2 16.0 %copy-start.34 = (f32[768]{0:T(1024)S(1)}, f32[768]{0:T(1024)}, u32[]{:S(2)}) copy-start(f32[768]{0:T(1024)} %get-tuple-element.181) | copy-start | bytes 9220
  160.2 3.9 %copy-start.47 = (f32[2,4]{1,0:T(2,128)S(1)}, f32[2,4]{1,0:T(2,128)}, u32[]{:S(2)}) copy-start(f32[2,4]{1,0:T(2,128)} %exponential_multiply_fusion.3) | copy-start | bytes 100
  162.1 18.8 %copy-start.20 = (bf16[128,128]{0,1:T(8,128)(2,1)}, bf16[128,128]{0,1:T(8,128)(2,1)S(1)}, u32[]{:S(2)}) copy-start(bf16[128,128]{0,1:T(8,128)(2,1)S(1)} %copy.166) | copy-start | bytes 98308
  181.5 25.4 %copy-start.3 = (f32[2,4,64,64]{3,2,1,0:T(8,128)}, f32[2,4,64,64]{3,2,1,0:T(8,128)S(1)}, u32[]{:S(2)}) copy-start(f32[2,4,64,64]{3,2,1,0:T(8,128)S(1)} %get-tuple-element.175) | copy-start | bytes 393220
  220.5 3.9 %copy-start.14 = (bf16[128,512]{0,1:T(8,128)(2,1)S(1)}, bf16[128,512]{0,1:T(8,128)(2,1)}, u32[]{:S(2)}) copy-start(bf16[128,512]{0,1:T(8,128)(2,1)} %copy.178) | copy-start | bytes 393220
  220.5 3.9 %copy-start.23 = (f32[128,128,2]{1,0,2:T(8,128)S(1)}, f32[128,128,2]{1,0,2:T(8,128)}, u32[]{:S(2)}) copy-start(f32[128,128,2]{1,0,2:T(8,128)} %copy.181) | copy-start | bytes 393220
  220.5 3.9 %copy-start.40 = (f32[128,8]{0,1:T(8,128)S(1)}, f32[128,8]{0,1:T(8,128)}, u32[]{:S(2)}) copy-start(f32[128,8]{0,1:T(8,128)} %rev.22) | copy-start | bytes 12292
  220.5 3.9 %copy-start.49 = (f32[128,2,4]{0,2,1:T(4,128)S(1)}, f32[128,2,4]{0,2,1:T(4,128)}, u32[]{:S(2)}) copy-start(f32[128,2,4]{0,2,1:T(4,128)} %copy.183) | copy-start | bytes 12292
  223.3 8.4 %copy-start.4 = (f32[2,4,64,64]{3,2,1,0:T(8,128)S(1)}, f32[2,4,64,64]{3,2,1,0:T(8,128)}, u32[]{:S(2)}) copy-start(f32[2,4,64,64]{3,2,1,0:T(8,128)} %copy-done.3) | copy-start | bytes 393220
  230.6 3.9 %copy-start.8 = (f32[128,512]{0,1:T(8,128)S(1)}, f32[128,512]{0,1:T(8,128)}, u32[]{:S(2)}) copy-start(f32[128,512]{0,1:T(8,128)} %copy.190) | copy-start | bytes 786436
  230.6 3.9 %copy-start.9 = (f32[128,2,4,64]{0,3,2,1:T(8,128)S(1)}, f32[128,2,4,64]{0,3,2,1:T(8,128)}, u32[]{:S(2)}) copy-start(f32[128,2,4,64]{0,3,2,1:T(8,128)} %rev.23) | copy-start | bytes 786436
  230.6 3.9 %copy-start.17 = (f32[128,128,2]{1,0,2:T(8,128)S(1)}, f32[128,128,2]{1,0,2:T(8,128)}, u32[]{:S(2)}) copy-start(f32[128,128,2]{1,0,2:T(8,128)} %copy.168) | copy-start | bytes 393220
  230.6 3.9 %copy-start.26 = (f32[128,8]{0,1:T(8,128)S(1)}, f32[128,8]{0,1:T(8,128)}, u32[]{:S(2)}) copy-start(f32[128,8]{0,1:T(8,128)} %copy-done.25) | copy-start | bytes 12292
  230.6 3.9 %copy-start.29 = (f32[128,2,4]{0,2,1:T(4,128)S(1)}, f32[128,2,4]{0,2,1:T(4,128)}, u32[]{:S(2)}) copy-start(f32[128,2,4]{0,2,1:T(4,128)} %copy.170) | copy-start | bytes 12292
  231.7 3.2 %copy-start.35 = (f32[2,4,64]{2,1,0:T(4,128)S(1)}, f32[2,4,64]{2,1,0:T(4,128)}, u32[]{:S(2)}) copy-start(f32[2,4,64]{2,1,0:T(4,128)} %reshape.218) | copy-start | bytes 6148
  234.5 9.5 %copy-start.7 = (bf16[64,2048]{1,0:T(8,128)(2,1)S(1)}, bf16[64,2048]{1,0:T(8,128)(2,1)}, u32[]{:S(2)}) copy-start(bf16[64,2048]{1,0:T(8,128)(2,1)} %param.22) | copy-start | bytes 786436
  234.9 9.1 %copy-start.30 = (f32[1,2048]{1,0:T(1,128)S(1)}, f32[1,2048]{1,0:T(1,128)}, u32[]{:S(2)}) copy-start(f32[1,2048]{1,0:T(1,128)} %get-tuple-element.226) | copy-start | bytes 24580
  (11 other events, 22.2 us)
where the time goes:
time: 250 us; the launch traced here: 248 us
  blocking collectives  122 us (49%)
  local copies, waits for them, and re-layouts  58.6 us (23%)
  other arithmetic  34.5 us (14%)
  matrix products  28.4 us (11%)
  starting transfers between devices  3.15 us (1%)
    all_gather x4, blocking collectives, prefix(): lax.all_gather(a.astype(kind), axis)  54.2 us
    psum x1, blocking collectives, local(): lax.psum(jnp.dot(own_cols, modulation, preferred_element_type=jnp.float32...  39.4 us
    all_gather x1, blocking collectives, local(): context_cols = lax.all_gather(own_context, 'sp', axis=0, tiled=True)  14.5 us
    dot_general x10, matrix products, project_many(): jnp.dot(row_block, weight, preferred_element_type=jnp.float32)  10.5 us
    all_gather x1, blocking collectives, local(): lax.all_gather(hidden, 'tp', axis=0, tiled=True)  7.17 us
    all_to_all x1, blocking collectives, local(): lax.all_to_all(stacked, 'tp', split_axis=0, concat_axis=2, tiled=True)[0]  6.85 us
    another operation x3, other arithmetic  6.56 us
    exp x4, local copies, waits for them, and re-layouts, directed_pass(): jnp.exp(running)  5.96 us
  transfers between devices with their start and end apart: 2, of which 0 were waited for; matrix products, arithmetic and copies ran while one was open for 28% of the time, Pallas kernels for 0%

commit v1 on v0

--- a/solution.py
+++ b/solution.py
@@ -2,6 +2,7 @@
 import jax.numpy as jnp
 from jax import lax
 from jax.sharding import PartitionSpec as P
+from jax.lax import axis_index, axis_size, ppermute
 
 HEAD_DIM = 64
 STATE = 64
@@ -240,7 +241,20 @@
     own_context = project_many(
         modulated_norm(context, norm_gain, shift_rows[1], scale_rows[1]), context_mats
     )
-    context_cols = lax.all_gather(own_context, "sp", axis=0, tiled=True)
+
+    def drive_bars(xin):
+        n_peers_all = axis_size("sp")
+        next_value = [None] * n_peers_all
+        steps_seen = [(ii, (ii + 1) % n_peers_all) for ii in range(n_peers_all)]
+        next_value[n_peers_all - 1] = xin
+        for tick in range(n_peers_all - 2, -1, -1):
+            next_value[tick] = ppermute(next_value[tick + 1], "sp", steps_seen)
+        prior = jnp.concatenate(next_value, axis=0)
+        now = axis_index("sp")
+        tall = (now + 1) * xin.shape[0]
+        return jnp.roll(prior, tall, axis=0)
+
+    context_cols = drive_bars(own_context)
     ctx_span = head_cols + state_cols
     ctx_padded = jnp.pad(context_cols[:, :ctx_span], ((2, 1), (0, 0)))
     ctx_conv = conv_padded(

time: 250 us -> 257 us (1.028)
  waiting for transfers between devices: 0.01 us -> 11.1 us
  blocking collectives: 122 us -> 112 us
  local copies, waits for them, and re-layouts: 58.6 us -> 63.6 us
    all_gather x1 -> x0, blocking collectives: 14.5 us -> none  [local(): context_cols = lax.all_gather(own_context, 'sp', axis=0, tiled=True)]
    ppermute x0 -> x3, waiting for transfers between devices: none -> 11.1 us  [drive_bars(): next_value[tick] = ppermute(next_value[tick + 1], 'sp', steps_seen)]
    all_gather x4, blocking collectives: 54.2 us -> 59.1 us  [prefix(): lax.all_gather(a.astype(kind), axis)]
  transfers between devices with their start and end apart: 2 -> 5, of which waited for: 0 -> 2; matrix products, arithmetic and copies ran while one was open for 28% -> 32% of each run, Pallas kernels for 0% -> 0%
where the time goes in v1:
time: 257 us; the launch traced here: 254 us
  blocking collectives  112 us (44%)
  local copies, waits for them, and re-layouts  63.6 us (25%)
  other arithmetic  35.3 us (14%)
  matrix products  28.1 us (11%)
  waiting for transfers between devices  11.1 us (4%)
  starting transfers between devices  3.22 us (1%)
    all_gather x4, blocking collectives, prefix(): lax.all_gather(a.astype(kind), axis)  59.1 us
    psum x1, blocking collectives, local(): lax.psum(jnp.dot(own_cols, modulation, preferred_element_type=jnp.float32...  39.3 us
    ppermute x3, waiting for transfers between devices, drive_bars(): next_value[tick] = ppermute(next_value[tick + 1], 'sp', steps_seen)  11.1 us
    dot_general x10, matrix products, project_many(): jnp.dot(row_block, weight, preferred_element_type=jnp.float32)  8 us
    another operation x3, other arithmetic  7.18 us
    all_gather x1, blocking collectives, local(): lax.all_gather(hidden, 'tp', axis=0, tiled=True)  7.04 us
    all_to_all x1, blocking collectives, local(): lax.all_to_all(stacked, 'tp', split_axis=0, concat_axis=2, tiled=True)[0]  6.85 us
    exp x4, local copies, waits for them, and re-layouts, directed_pass(): jnp.exp(running)  5.93 us
  transfers between devices with their start and end apart: 5, of which 2 were waited for; matrix products, arithmetic and copies ran while one was open for 32% of the time, Pallas kernels for 0%

profile of v1, /device:TPU:0, one launch (start us, length us, event | category | flops | bytes accessed | tf_op | source)
XLA Modules:
  0.0 254.4 jit_solution(6130015616322045516)
XLA Ops:
  2.4 39.3 %psum.7 = f32[2,6144]{1,0:T(2,128)S(1)} all-reduce(f32[2,6144]{1,0:T(2,128)S(1)} %fusion.93), channel_id=1, replica_groups=mesh['sp'=4,'tp'=2,'dp'=4] {'sp','tp'}, use_global_device_ids=true, to_apply=%region_0.1 | all-reduce | flops 12288 | bytes 98304 | tf_op jit(solution)/shard_map/psum | solution.py:210
  43.7 1.6 convolution_convert_fusion.6
  48.2 7.0 %all_gather.23 = bf16[128,2048]{1,0:T(8,128)(2,1)S(1)} all-gather(bf16[64,2048]{1,0:T(8,128)(2,1)S(1)} %fusion.31), channel_id=1, replica_groups=mesh['sp'=4,'tp'=2,'dp'=4] {'tp'}, dimensions={0}, use_global_device_ids=true | all-gather | bytes 786432 | tf_op jit(solution)/shard_map/all_gather | solution.py:223
  57.4 1.9 collective-permute-start
  73.3 1.6 reduce_window_sum.52
  76.2 1.5 copy.188
  77.7 1.6 reduce_window_sum.56
  80.6 3.0 %divide_multiply_fusion = f32[128,512]{1,0:T(8,128)} fusion(bf16[128,2048]{1,0:T(8,128)(2,1)} %copy-done.1, bf16[2048,512]{1,0:T(8,128)(2,1)} %param.29), kind=kOutput, calls=%fused_computation.89 | convolution fusion | flops 268828672 | bytes 2883584 | tf_op jit(solution)/shard_map/dot_general | solution.py:64
  85.2 14.9 %all_gather.24 = bf16[4,2,4]{2,1,0:T(2,128)(2,1)} all-gather(bf16[1,2,4]{2,1,0:T(2,128)(2,1)S(1)} %copy-done.55), channel_id=1, replica_groups=mesh['sp'=4,'tp'=2,'dp'=4] {'sp'}, dimensions={0}, use_global_device_ids=true | all-gather | bytes 80 | tf_op jit(solution)/shard_map/all_gather | solution.py:20
  100.1 7.6 %all_gather.27 = bf16[4,2,4]{2,1,0:T(2,128)(2,1)} all-gather(bf16[1,2,4]{2,1,0:T(2,128)(2,1)S(1)} %copy-done.56), channel_id=1, replica_groups=mesh['sp'=4,'tp'=2,'dp'=4] {'sp'}, dimensions={0}, use_global_device_ids=true | all-gather | bytes 80 | tf_op jit(solution)/shard_map/all_gather | solution.py:20
  107.7 1.5 exp.128
  109.2 1.5 exp.139
  112.0 1.6 copy.176
  113.6 1.5 copy.174
  115.1 1.6 copy.189
  116.7 1.5 copy.187
  118.2 1.6 copy.185
  119.7 1.6 copy.172
  121.3 1.8 copy.190
  128.6 1.4 rev.19
  130.0 1.5 copy.167
  131.4 1.4 rev.20
  133.7 15.4 %all-gather = bf16[8,4,64,64]{3,2,1,0:T(8,128)(2,1)} all-gather(bf16[2,4,64,64]{3,2,1,0:T(8,128)(2,1)S(1)} %fusion.17), channel_id=2, replica_groups=mesh['sp'=4,'tp'=2,'dp'=4] {'sp'}, dimensions={0}, use_global_device_ids=true | all-gather | bytes 327680 | tf_op jit(solution)/shard_map/all_gather | solution.py:20
  151.0 1.7 copy.178
  152.7 1.5 copy.179
  156.0 21.2 %all-gather.1 = bf16[8,4,64,64]{3,2,1,0:T(8,128)(2,1)} all-gather(bf16[2,4,64,64]{3,2,1,0:T(8,128)(2,1)S(1)} %fusion.18), channel_id=3, replica_groups=mesh['sp'=4,'tp'=2,'dp'=4] {'sp'}, dimensions={0}, use_global_device_ids=true | all-gather | bytes 327680 | tf_op jit(solution)/shard_map/all_gather | solution.py:20
  178.5 9.1 %while.7 = (s32[]{:T(128)}, f32[2,4]{1,0:T(2,128)}, f32[2,4,64,64]{3,2,1,0:T(8,128)}, s32[]{:T(128)}, bf16[4,2,4]{2,1,0:T(2,128)(2,1)}, /*index=5*/bf16[4,2,4,64...) while((s32[]{:T(128)}, f32[2,4]{1,0:T(2,128)}, f32[2,4,64,64]{3,2,1,0:T(8,128)}, ...), condition=%wide.region_12.13_spmd, body=%wide.region_11.12_spmd.sunk | while | flops 98326 | bytes 327979 | solution.py:37
  179.8 1.8 convert_add_fusion.7
  182.8 1.8 convert_add_fusion.7
  185.8 1.8 convert_add_fusion.7
  188.9 1.5 copy.180
  190.3 1.6 convolution_bitcast_fusion.6
  192.0 1.7 copy.181
  193.6 1.6 convolution_bitcast_fusion.7
  195.3 1.6 copy.168
  197.0 1.7 fusion.11
  198.7 5.6 %collective-permute-done.3 = bf16[128,656]{0,1:T(8,128)(2,1)S(1)} collective-permute-done((bf16[128,656]{0,1:T(8,128)(2,1)}, bf16[128,656]{0,1:T(8,128)(2,1)S(1)}, u32[]{:S(2)}, u32[]{:S(2)}) %collective-permute-start.3) | collective-permute-done | bytes 167968 | tf_op jit(solution)/shard_map/ppermute | solution.py:251
  204.4 1.7 fusion.13
  206.1 5.4 %collective-permute-done.4 = bf16[128,656]{0,1:T(8,128)(2,1)S(1)} collective-permute-done((bf16[128,656]{0,1:T(8,128)(2,1)S(1)}, bf16[128,656]{0,1:T(8,128)(2,1)S(1)}, u32[]{:S(2)}, u32[]{:S(2)}) %collective-permute-start.4) | collective-permute-done | bytes 167968 | tf_op jit(solution)/shard_map/ppermute | solution.py:251
  216.2 1.6 multiply_convert_fusion
  218.7 5.1 %reduce-window.6 = f32[2,8,4,128]{3,1,2,0:T(8,128)} reduce-window(f32[2,8,4,128]{3,1,2,0:T(8,128)} %fusion.148, f32[]{:T(128)} %constant.148.clone.1), window={size=1x1x1x128 pad=0_0x0_0x0_0x127_0}, to_apply=%region_7.8 | reduce-window | flops 1040384 | bytes 65540 | tf_op jit(solution)/shard_map/reduce-window
  223.8 1.5 slice_reduce_fusion
  228.3 1.4 fusion.76
  232.4 1.8 fusion.15
  236.4 1.8 rev.23
  238.2 1.8 fusion.16
  243.6 6.8 %all_to_all.15 = bf16[2,64,512]{2,1,0:T(8,128)(2,1)S(1)} all-to-all(bf16[2,64,512]{2,1,0:T(8,128)(2,1)S(1)} %copy.199), channel_id=1, replica_groups=mesh['sp'=4,'tp'=2,'dp'=4] {'tp'}, dimensions={0} | all-to-all | bytes 262144 | tf_op jit(solution)/shard_map/all_to_all | solution.py:295
  250.7 3.8 %fusion.1 = bf16[64,2048]{1,0:T(8,128)(2,1)} fusion(bf16[64,1024]{1,0:T(8,128)(2,1)S(1)} %bitcast.213, bf16[1024,2048]{1,0:T(8,128)(2,1)} %param.39, bf16[64,2048]{1,0:T(8,128)(2,1)S(1)} %copy-done.3, f32[2048]{0:T(1024)S(1)} %bitcast.239), kind=kOutput, calls=%fused_computation.10 | convolution fusion | flops 268959744 | bytes 4857856 | tf_op jit(solution)/shard_map/dot_general | solution.py:294
  (227 shorter events, 62.1 us)
Async XLA Ops:
  1.9 40.5 %copy-start.49 = (bf16[2048]{0:T(1024)(128)(2,1)S(1)}, bf16[2048]{0:T(1024)(128)(2,1)}, u32[]{:S(2)}) copy-start(bf16[2048]{0:T(1024)(128)(2,1)} %param.27) | copy-start | bytes 12292
  1.9 41.7 %copy-start.30 = (bf16[2,2048,8]{1,2,0:T(8,128)(2,1)S(1)}, bf16[2,2048,8]{1,2,0:T(8,128)(2,1)}, u32[]{:S(2)}) copy-start(bf16[2,2048,8]{1,2,0:T(8,128)(2,1)} %param.32) | copy-start | bytes 196612
  41.8 3.5 %copy-start.14 = (bf16[128,2048]{1,0:T(8,128)(2,1)S(1)}, bf16[128,2048]{1,0:T(8,128)(2,1)}, u32[]{:S(2)}) copy-start(bf16[128,2048]{1,0:T(8,128)(2,1)} %param.24) | copy-start | bytes 1572868
  43.6 2.0 copy-start.4
  47.9 149.1 %collective-permute-start.2 = (bf16[128,656]{0,1:T(8,128)(2,1)}, bf16[128,656]{0,1:T(8,128)(2,1)}, u32[]{:S(2)}, u32[]{:S(2)}) collective-permute-start(bf16[128,656]{0,1:T(8,128)(2,1)} %pad_maximum_fusion), channel_id=1, source_target_pairs={{0,8},{8,16},{16,24},{24,0},{1,9},{9,17},{17,25},{25,1},{2,10},{10... | collective-permute-start | bytes 503816 | tf_op jit(solution)/shard_map/ppermute | solution.py:251
  55.2 5.6 %copy-start.1 = (bf16[128,2048]{1,0:T(8,128)(2,1)}, bf16[128,2048]{1,0:T(8,128)(2,1)S(1)}, u32[]{:S(2)}) copy-start(bf16[128,2048]{1,0:T(8,128)(2,1)S(1)} %all_gather.23) | copy-start | bytes 1572868
  55.7 5.1 %copy-start.7 = (bf16[128,512]{1,0:T(8,128)(2,1)}, bf16[128,512]{1,0:T(8,128)(2,1)S(1)}, u32[]{:S(2)}) copy-start(bf16[128,512]{1,0:T(8,128)(2,1)S(1)} %convolution_convert_fusion.2) | copy-start | bytes 393220
  56.5 5.4 %copy-start.21 = (bf16[128,128]{1,0:T(8,128)(2,1)}, bf16[128,128]{1,0:T(8,128)(2,1)S(1)}, u32[]{:S(2)}) copy-start(bf16[128,128]{1,0:T(8,128)(2,1)S(1)} %convolution_convert_fusion.5) | copy-start | bytes 98308
  56.5 4.6 %copy-start.54 = (f32[2,8]{1,0:T(2,128)S(1)}, f32[2,8]{1,0:T(2,128)}, u32[]{:S(2)}) copy-start(f32[2,8]{1,0:T(2,128)} %param.36) | copy-start | bytes 196
  56.5 4.7 %copy-start.53 = (f32[128,8]{0,1:T(8,128)S(1)}, f32[128,8]{0,1:T(8,128)}, u32[]{:S(2)}) copy-start(f32[128,8]{0,1:T(8,128)} %param.37) | copy-start | bytes 12292
  56.8 5.1 %copy-start.22 = (bf16[128,128]{1,0:T(8,128)(2,1)}, bf16[128,128]{1,0:T(8,128)(2,1)S(1)}, u32[]{:S(2)}) copy-start(bf16[128,128]{1,0:T(8,128)(2,1)S(1)} %convolution_convert_fusion.4) | copy-start | bytes 98308
  57.4 67.1 %collective-permute-start = (bf16[2,768]{1,0:T(2,128)(2,1)}, bf16[2,768]{1,0:T(2,128)(2,1)}, u32[]{:S(2)}, u32[]{:S(2)}) collective-permute-start(bf16[2,768]{1,0:T(2,128)(2,1)} %get-tuple-element.220), channel_id=1, source_target_pairs={{0,8},{8,16},{16,24},{1,9},{9,17},{17,25},{2,10},{10,18},{18,26},{... | collective-permute-start | bytes 9224 | tf_op jit(solution)/shard_map/ppermute | solution.py:45
  59.3 65.2 %collective-permute-start.1 = (bf16[2,768]{1,0:T(2,128)(2,1)}, bf16[2,768]{1,0:T(2,128)(2,1)}, u32[]{:S(2)}, u32[]{:S(2)}) collective-permute-start(bf16[2,768]{1,0:T(2,128)(2,1)} %get-tuple-element.221), channel_id=1, source_target_pairs={{8,0},{16,8},{24,16},{9,1},{17,9},{25,17},{10,2},{18,10},{26,18},{... | collective-permute-start | bytes 9224 | tf_op jit(solution)/shard_map/ppermute | solution.py:48
  60.9 22.8 %copy-start.28 = (f32[128,8]{0,1:T(8,128)}, f32[128,8]{0,1:T(8,128)S(1)}, u32[]{:S(2)}) copy-start(f32[128,8]{0,1:T(8,128)S(1)} %compare_select_fusion.3) | copy-start | bytes 12292
  80.6 3.0 %copy-start.51 = (f32[2,4]{1,0:T(2,128)S(1)}, f32[2,4]{1,0:T(2,128)}, u32[]{:S(2)}) copy-start(f32[2,4]{1,0:T(2,128)} %slice_bitcast_fusion.3) | copy-start | bytes 100
  80.6 3.0 %copy-start.18 = (f32[128,2,4]{2,1,0:T(2,128)S(1)}, f32[128,2,4]{2,1,0:T(2,128)}, u32[]{:S(2)}) copy-start(f32[128,2,4]{2,1,0:T(2,128)} %copy.175) | copy-start | bytes 12292
  80.6 3.8 %copy-start.52 = (f32[2,4]{1,0:T(2,128)S(1)}, f32[2,4]{1,0:T(2,128)}, u32[]{:S(2)}) copy-start(f32[2,4]{1,0:T(2,128)} %slice_bitcast_fusion.2) | copy-start | bytes 100
  80.6 3.8 %copy-start.19 = (f32[128,2,4]{2,1,0:T(2,128)S(1)}, f32[128,2,4]{2,1,0:T(2,128)}, u32[]{:S(2)}) copy-start(f32[128,2,4]{2,1,0:T(2,128)} %copy.188) | copy-start | bytes 12292
  80.6 4.6 %copy-start.55 = (bf16[1,2,4]{2,1,0:T(2,128)(2,1)S(1)}, bf16[1,2,4]{2,1,0:T(2,128)(2,1)}, u32[]{:S(2)}) copy-start(bf16[1,2,4]{2,1,0:T(2,128)(2,1)} %convert_element_type.233) | copy-start | bytes 52
  80.6 19.5 %copy-start.56 = (bf16[1,2,4]{2,1,0:T(2,128)(2,1)S(1)}, bf16[1,2,4]{2,1,0:T(2,128)(2,1)}, u32[]{:S(2)}) copy-start(bf16[1,2,4]{2,1,0:T(2,128)(2,1)} %convert_element_type.248) | copy-start | bytes 52
  111.3 13.2 %copy-start.8 = (bf16[128,512]{1,0:T(8,128)(2,1)S(1)}, bf16[128,512]{1,0:T(8,128)(2,1)}, u32[]{:S(2)}) copy-start(bf16[128,512]{1,0:T(8,128)(2,1)} %copy-done.7) | copy-start | bytes 393220
  112.0 13.3 %copy-start.37 = (f32[768]{0:T(1024)S(1)}, f32[768]{0:T(1024)}, u32[]{:S(2)}) copy-start(f32[768]{0:T(1024)} %get-tuple-element.178) | copy-start | bytes 9220
  112.0 13.3 %copy-start.38 = (f32[768]{0:T(1024)S(1)}, f32[768]{0:T(1024)}, u32[]{:S(2)}) copy-start(f32[768]{0:T(1024)} %get-tuple-element.179) | copy-start | bytes 9220
  112.0 13.3 %copy-start.39 = (f32[768]{0:T(1024)S(1)}, f32[768]{0:T(1024)}, u32[]{:S(2)}) copy-start(f32[768]{0:T(1024)} %get-tuple-element.180) | copy-start | bytes 9220
  112.0 13.3 %copy-start.40 = (f32[768]{0:T(1024)S(1)}, f32[768]{0:T(1024)}, u32[]{:S(2)}) copy-start(f32[768]{0:T(1024)} %get-tuple-element.181) | copy-start | bytes 9220
  126.4 22.8 %copy-start.5 = (bf16[128,512]{0,1:T(8,128)(2,1)}, bf16[128,512]{0,1:T(8,128)(2,1)S(1)}, u32[]{:S(2)}) copy-start(bf16[128,512]{0,1:T(8,128)(2,1)S(1)} %copy.165) | copy-start | bytes 393220
  128.6 20.6 %copy-start.23 = (bf16[128,128]{0,1:T(8,128)(2,1)}, bf16[128,128]{0,1:T(8,128)(2,1)S(1)}, u32[]{:S(2)}) copy-start(bf16[128,128]{0,1:T(8,128)(2,1)S(1)} %copy.166) | copy-start | bytes 98308
  196.9 15.7 %copy-start.25 = (bf16[128,128]{0,1:T(8,128)(2,1)S(1)}, bf16[128,128]{0,1:T(8,128)(2,1)}, u32[]{:S(2)}) copy-start(bf16[128,128]{0,1:T(8,128)(2,1)} %copy-done.24) | copy-start | bytes 98308
  196.9 15.7 %copy-start.34 = (bf16[128,8]{0,1:T(8,128)(2,1)S(1)}, bf16[128,8]{0,1:T(8,128)(2,1)}, u32[]{:S(2)}) copy-start(bf16[128,8]{0,1:T(8,128)(2,1)} %copy-done.33) | copy-start | bytes 6148
  196.9 15.7 %copy-start.36 = (bf16[128,8]{0,1:T(8,128)(2,1)S(1)}, bf16[128,8]{0,1:T(8,128)(2,1)}, u32[]{:S(2)}) copy-start(bf16[128,8]{0,1:T(8,128)(2,1)} %copy-done.35) | copy-start | bytes 6148
  196.9 7.4 %collective-permute-start.3 = (bf16[128,656]{0,1:T(8,128)(2,1)}, bf16[128,656]{0,1:T(8,128)(2,1)S(1)}, u32[]{:S(2)}, u32[]{:S(2)}) collective-permute-start(bf16[128,656]{0,1:T(8,128)(2,1)} %collective-permute-done.2), channel_id=1, source_target_pairs={{0,8},{8,16},{16,24},{24,0},{1,9},{9,17},{17,25},{25,1},{2,10},{10... | collective-permute-start | bytes 503816 | tf_op jit(solution)/shard_map/ppermute | solution.py:251
  204.4 7.2 %collective-permute-start.4 = (bf16[128,656]{0,1:T(8,128)(2,1)S(1)}, bf16[128,656]{0,1:T(8,128)(2,1)S(1)}, u32[]{:S(2)}, u32[]{:S(2)}) collective-permute-start(bf16[128,656]{0,1:T(8,128)(2,1)S(1)} %collective-permute-done.3), channel_id=1, source_target_pairs={{0,8},{8,16},{16,24},{24,0},{1,9},{9,17},{17,25},{25,1},{2,10},{10... | collective-permute-start | bytes 503816 | tf_op jit(solution)/shard_map/ppermute | solution.py:251
  206.1 7.8 %copy-start.43 = (f32[2,8]{1,0:T(2,128)S(1)}, f32[2,8]{1,0:T(2,128)}, u32[]{:S(2)}) copy-start(f32[2,8]{1,0:T(2,128)} %copy-done.42) | copy-start | bytes 196
  218.7 16.5 %copy-start.9 = (bf16[512,128]{0,1:T(8,128)(2,1)}, bf16[512,128]{0,1:T(8,128)(2,1)S(1)}, u32[]{:S(2)}) copy-start(bf16[512,128]{0,1:T(8,128)(2,1)S(1)} %slice.228) | copy-start | bytes 393220
  232.4 2.9 %copy-start.17 = (bf16[128,512]{0,1:T(8,128)(2,1)S(1)}, bf16[128,512]{0,1:T(8,128)(2,1)}, u32[]{:S(2)}) copy-start(bf16[128,512]{0,1:T(8,128)(2,1)} %copy.178) | copy-start | bytes 393220
  232.4 2.9 %copy-start.26 = (f32[128,2,4,64]{0,3,2,1:T(8,128)S(1)}, f32[128,2,4,64]{0,3,2,1:T(8,128)}, u32[]{:S(2)}) copy-start(f32[128,2,4,64]{0,3,2,1:T(8,128)} %fusion.11) | copy-start | bytes 786436
  232.4 2.9 %copy-start.27 = (f32[128,128,2]{1,0,2:T(8,128)S(1)}, f32[128,128,2]{1,0,2:T(8,128)}, u32[]{:S(2)}) copy-start(f32[128,128,2]{1,0,2:T(8,128)} %copy.181) | copy-start | bytes 393220
  232.4 2.9 %copy-start.44 = (f32[128,8]{0,1:T(8,128)S(1)}, f32[128,8]{0,1:T(8,128)}, u32[]{:S(2)}) copy-start(f32[128,8]{0,1:T(8,128)} %rev.22) | copy-start | bytes 12292
  232.4 2.9 %copy-start.50 = (f32[128,2,4]{0,2,1:T(4,128)S(1)}, f32[128,2,4]{0,2,1:T(4,128)}, u32[]{:S(2)}) copy-start(f32[128,2,4]{0,2,1:T(4,128)} %copy.183) | copy-start | bytes 12292
  236.4 4.7 %copy-start.6 = (bf16[128,512]{0,1:T(8,128)(2,1)S(1)}, bf16[128,512]{0,1:T(8,128)(2,1)}, u32[]{:S(2)}) copy-start(bf16[128,512]{0,1:T(8,128)(2,1)} %copy-done.5) | copy-start | bytes 393220
  238.2 2.9 %copy-start.10 = (f32[128,512]{0,1:T(8,128)S(1)}, f32[128,512]{0,1:T(8,128)}, u32[]{:S(2)}) copy-start(f32[128,512]{0,1:T(8,128)} %copy.190) | copy-start | bytes 786436
  238.2 2.9 %copy-start.11 = (f32[128,2,4,64]{0,3,2,1:T(8,128)S(1)}, f32[128,2,4,64]{0,3,2,1:T(8,128)}, u32[]{:S(2)}) copy-start(f32[128,2,4,64]{0,3,2,1:T(8,128)} %fusion.13) | copy-start | bytes 786436
  238.2 2.9 %copy-start.12 = (f32[128,2,4,64]{0,3,2,1:T(8,128)S(1)}, f32[128,2,4,64]{0,3,2,1:T(8,128)}, u32[]{:S(2)}) copy-start(f32[128,2,4,64]{0,3,2,1:T(8,128)} %rev.23) | copy-start | bytes 786436
  238.2 2.9 %copy-start.20 = (f32[128,128,2]{1,0,2:T(8,128)S(1)}, f32[128,128,2]{1,0,2:T(8,128)}, u32[]{:S(2)}) copy-start(f32[128,128,2]{1,0,2:T(8,128)} %copy.168) | copy-start | bytes 393220
  238.2 2.9 %copy-start.29 = (f32[128,8]{0,1:T(8,128)S(1)}, f32[128,8]{0,1:T(8,128)}, u32[]{:S(2)}) copy-start(f32[128,8]{0,1:T(8,128)} %copy-done.28) | copy-start | bytes 12292
  238.2 2.9 %copy-start.31 = (f32[128,2,4]{0,2,1:T(4,128)S(1)}, f32[128,2,4]{0,2,1:T(4,128)}, u32[]{:S(2)}) copy-start(f32[128,2,4]{0,2,1:T(4,128)} %copy.170) | copy-start | bytes 12292
  241.5 9.1 %copy-start.3 = (bf16[64,2048]{1,0:T(8,128)(2,1)S(1)}, bf16[64,2048]{1,0:T(8,128)(2,1)}, u32[]{:S(2)}) copy-start(bf16[64,2048]{1,0:T(8,128)(2,1)} %param.22) | copy-start | bytes 786436
  241.5 9.1 %copy-start.32 = (f32[1,2048]{1,0:T(1,128)S(1)}, f32[1,2048]{1,0:T(1,128)}, u32[]{:S(2)}) copy-start(f32[1,2048]{1,0:T(1,128)} %get-tuple-element.226) | copy-start | bytes 24580
  (14 other events, 16.3 us)
